TPU v7x, 32 devices: a whole 2x2x4 slice. The times are simulated.
32 devices in a mesh: sp: 8 (over z, y), tp: 4 (over x, core).
Axes of the slice: x: 2, y: 2, z: 4, core: 2. Of those that a mesh axis runs over, the one named last changes fastest.
Arguments:
- query_rows: bfloat16 [2048, 2048], P('sp', 'tp'), may hold values from -5.5 to 5.5
- key_rows: bfloat16 [2048, 2048], P('sp', 'tp'), may hold values from -5.5 to 5.5
- value_rows: bfloat16 [2048, 2048], P('sp', 'tp'), may hold values from -6 to 6
- out_grad: bfloat16 [2048, 2048], P('sp', 'tp'), may hold values from -96 to 96
- rel_bias: float32 [256, 32], replicated, may hold values from -3 to 3
Outputs:
- query_grad: bfloat16 [2048, 2048], P('sp', 'tp')
- key_grad: bfloat16 [2048, 2048], P('sp', 'tp')
- value_grad: bfloat16 [2048, 2048], P('sp', 'tp')
- table_grad: float32 [256, 32], P('sp')
All inputs are finite; a program needn't handle non-finite values.
Results may differ from a plain program's by a relative error of at most 0.007.
Values may be sent and summed in bfloat16 or wider, within the bound.
A program may use at most 64 MiB of HBM per device.

v0:
```python
from functools import partial

import jax
import jax.numpy as jnp
from jax import lax
from jax.sharding import PartitionSpec as P

HEAD_DIM = 64
SEG = 64
LEFT = 4
CLIP = 128


NEG_FILL = -1e30


def passed_along(block, axis, distance):
    devices = range(lax.axis_size(axis))
    route = [(i - distance, i) for i in devices if i - distance in devices]
    return lax.ppermute(block, axis, route)


def banded(extended, seg_count, seg_len, band_len):
    layers = []
    for offset in range(band_len // seg_len):
        window = lax.slice_in_dim(
            extended, offset * seg_len, offset * seg_len + seg_count * seg_len, axis=0
        )
        layers.append(window.reshape((seg_count, 1, seg_len) + extended.shape[1:]))
    return jnp.concatenate(layers, axis=1).reshape((seg_count, band_len) + extended.shape[1:])


def unbanded(band_grads, ext_len, seg_len):
    seg_count, band_len = (band_grads.shape[0], band_grads.shape[1])
    trailing = band_grads.shape[2:]
    blocks = band_grads.reshape((seg_count, band_len // seg_len, seg_len) + trailing)
    summed = jnp.zeros((ext_len,) + trailing, band_grads.dtype)
    for offset in range(band_len // seg_len):
        stripe = blocks[:, offset].reshape((seg_count * seg_len,) + trailing)
        widths = [(offset * seg_len, ext_len - offset * seg_len - seg_count * seg_len)] + [
            (0, 0)
        ] * len(trailing)
        summed = summed + jnp.pad(stripe, widths)
    return summed


def diagonal_sums(square, rel_top, table_rows, clip_half):
    row_count, col_count = square.shape
    flipped = square[::-1]
    padded = jnp.pad(flipped, ((0, 0), (0, row_count)))
    sheared = padded.reshape(-1)[: row_count * (col_count + row_count - 1)].reshape(
        row_count, col_count + row_count - 1
    )
    diagonals = jnp.sum(sheared, axis=0)
    relative = rel_top - jnp.arange(col_count + row_count - 1, dtype=jnp.int32)
    bin_index = jnp.clip(relative, -clip_half, clip_half - 1) + clip_half
    onehot = bin_index[:, None] == jnp.arange(table_rows, dtype=jnp.int32)[None, :]
    return jnp.sum(jnp.where(onehot, diagonals[:, None], 0.0), axis=0)


def segment_grads(query_segs, dout_segs, key_ext, value_ext, key_valid, bias_band):
    seg_len, band_len = bias_band.shape
    seg_count = query_segs.shape[0]
    score_scale = query_segs.shape[-1] ** (-0.5)
    key_band = banded(key_ext, seg_count, seg_len, band_len)
    value_band = banded(value_ext, seg_count, seg_len, band_len)
    valid_band = banded(key_valid, seg_count, seg_len, band_len)
    scores = (
        jnp.einsum("jid,jcd->jic", query_segs, key_band, preferred_element_type=jnp.float32)
        * score_scale
        + bias_band[None]
    )
    scores = jnp.where(valid_band[:, None, :], scores, NEG_FILL)
    row_peak = jnp.max(scores, axis=-1)
    log_norm = row_peak + jnp.log(jnp.sum(jnp.exp(scores - row_peak[..., None]), axis=-1))
    attention = jnp.exp(scores - log_norm[..., None])
    attention_half = attention.astype(jnp.bfloat16)
    attention_grad = jnp.einsum(
        "jie,jce->jic", dout_segs, value_band, preferred_element_type=jnp.float32
    )
    inner_sums = jnp.sum(attention * attention_grad, axis=-1)
    dscores = attention * (attention_grad - inner_sums[..., None])
    dscore_half = dscores.astype(jnp.bfloat16)
    dquery = (
        jnp.einsum("jic,jcd->jid", dscore_half, key_band, preferred_element_type=jnp.float32)
        * score_scale
    )
    dkey_band = (
        jnp.einsum("jic,jid->jcd", dscore_half, query_segs, preferred_element_type=jnp.float32)
        * score_scale
    )
    dvalue_band = jnp.einsum(
        "jic,jie->jce", attention_half, dout_segs, preferred_element_type=jnp.float32
    )
    ext_len = key_ext.shape[0]
    return (
        dquery,
        unbanded(dkey_band, ext_len, seg_len),
        unbanded(dvalue_band, ext_len, seg_len),
        jnp.sum(dscores, axis=0),
        log_norm,
        inner_sums,
    )


def by_heads(row_block):
    return jnp.transpose(
        row_block.reshape(row_block.shape[0], row_block.shape[1] // HEAD_DIM, HEAD_DIM), (1, 0, 2)
    )


def from_heads(stacked):
    return jnp.transpose(stacked, (1, 0, 2)).reshape(
        stacked.shape[1], stacked.shape[0] * stacked.shape[2]
    )


def shards(query_rows, key_rows, value_rows, out_grad, rel_bias):
    tok_rows, width_here = query_rows.shape
    heads_here = width_here // HEAD_DIM
    reach_rows = LEFT * SEG
    band_len = reach_rows + SEG
    seg_count = tok_rows // SEG
    distance = 1
    received = [passed_along((key_rows, value_rows), "sp", distance)]
    halo_keys = jnp.concatenate([arrived[0] for arrived in received], axis=0)
    halo_values = jnp.concatenate([arrived[1] for arrived in received], axis=0)
    key_ext = jnp.concatenate([halo_keys, key_rows], axis=0)
    value_ext = jnp.concatenate([halo_values, value_rows], axis=0)
    first_row = lax.axis_index("sp") * tok_rows - reach_rows
    key_valid = first_row + jnp.arange(reach_rows + tok_rows, dtype=jnp.int32) >= 0
    table_here = lax.dynamic_slice_in_dim(
        rel_bias, lax.axis_index("tp") * heads_here, heads_here, 1
    )
    row_pos = jnp.arange(SEG, dtype=jnp.int32)[:, None]
    col_pos = jnp.arange(band_len, dtype=jnp.int32)[None, :]
    offset_index = jnp.clip(reach_rows + row_pos - col_pos, -CLIP, CLIP - 1) + CLIP
    bias_bands = jnp.transpose(jnp.take(table_here, offset_index, axis=0), (2, 0, 1))

    def own_head(inputs):
        query_head, dout_head, key_head, value_head, bias_band = inputs
        return segment_grads(
            query_head.reshape(seg_count, SEG, HEAD_DIM),
            dout_head.reshape(seg_count, SEG, HEAD_DIM),
            key_head,
            value_head,
            key_valid,
            bias_band,
        )

    dquery, dkey_ext, dvalue_ext, squares, log_norm, inner_sums = lax.map(
        own_head,
        (
            by_heads(query_rows),
            by_heads(out_grad),
            by_heads(key_ext),
            by_heads(value_ext),
            bias_bands,
        ),
    )
    query_grad = from_heads(dquery.reshape(heads_here, tok_rows, HEAD_DIM)).astype(jnp.bfloat16)
    key_total = from_heads(dkey_ext[:, reach_rows:])
    value_total = from_heads(dvalue_ext[:, reach_rows:])
    table_terms = jnp.transpose(
        jax.vmap(
            partial(
                diagonal_sums, rel_top=reach_rows + SEG - 1, table_rows=2 * CLIP, clip_half=CLIP
            )
        )(squares)
    )
    back_keys = from_heads(dkey_ext[:, :reach_rows])
    back_values = from_heads(dvalue_ext[:, :reach_rows])
    distance = 1
    arrived = (
        passed_along(back_keys.astype(jnp.bfloat16), "sp", -distance).astype(back_keys.dtype),
        passed_along(back_values.astype(jnp.bfloat16), "sp", -distance).astype(back_values.dtype),
    )
    key_total = key_total + arrived[0]
    value_total = value_total + arrived[1]
    partial_rows = lax.psum_scatter(table_terms, "sp", scatter_dimension=0, tiled=True)
    table_grad = lax.all_gather(partial_rows, "tp", axis=1, tiled=True)
    return (
        query_grad,
        key_total.astype(jnp.bfloat16),
        value_total.astype(jnp.bfloat16),
        table_grad,
    )


def solution(mesh):
    return jax.shard_map(
        shards,
        mesh=mesh,
        in_specs=(P("sp", "tp"), P("sp", "tp"), P("sp", "tp"), P("sp", "tp"), P()),
        out_specs=(P("sp", "tp"), P("sp", "tp"), P("sp", "tp"), P("sp", None)),
        check_vma=False,
    )
```

profile of v0, /device:TPU:0, one launch (start us, length us, event | category | flops | bytes accessed | tf_op | source)
XLA Modules:
  0.0 248.5 jit_solution(1393977973975553837)
XLA Ops:
  7.2 1.1 copy.207
  8.3 4.9 %collective-permute-start = (bf16[256,512]{0,1:T(8,128)(2,1)S(1)}, bf16[256,512]{0,1:T(8,128)(2,1)S(1)}, u32[]{:S(2)}, u32[]{:S(2)}) collective-permute-start(bf16[256,512]{0,1:T(8,128)(2,1)S(1)} %copy.207), channel_id=1, source_target_pairs={{0,4},{4,8},{8,12},{12,16},{16,20},{20,24},{24,28},{1,5},{5,9},{9,... | collective-permute-start | bytes 786440 | tf_op jit(solution)/shard_map/ppermute | solution.py:20
  13.2 1.1 copy.212
  14.3 3.4 %collective-permute-start.1 = (bf16[256,512]{0,1:T(8,128)(2,1)S(1)}, bf16[256,512]{0,1:T(8,128)(2,1)S(1)}, u32[]{:S(2)}, u32[]{:S(2)}) collective-permute-start(bf16[256,512]{0,1:T(8,128)(2,1)S(1)} %copy.212), channel_id=1, source_target_pairs={{0,4},{4,8},{8,12},{12,16},{16,20},{20,24},{24,28},{1,5},{5,9},{9,... | collective-permute-start | bytes 786440 | tf_op jit(solution)/shard_map/ppermute | solution.py:20
  18.3 68.1 %gather_fusion = f32[20480,8]{1,0:T(8,128)} fusion(f32[256,8]{1,0:T(8,128)S(1)} %copy.245, s32[20480]{0:T(1024)S(1)} %broadcast_clamp_fusion), kind=kCustom, calls=%fused_computation | custom fusion | bytes 1392640 | tf_op jit(solution)/shard_map/jit(_take)/gather | solution.py:138
  86.4 6.3 %copy.210 = f32[64,320,8]{1,0,2:T(8,128)S(1)} copy(f32[64,320,8]{2,1,0:T(8,128)} %bitcast.234) | data formatting | bytes 1310720 | tf_op jit(solution)/shard_map/jit(_take)/gather | solution.py:138
  92.7 1.0 select_bitcast_fusion
  94.0 0.8 copy.211
  94.9 0.8 iota_compare_fusion
  95.8 64.9 %while.19 = (s32[]{:T(128)}, bf16[8,4,64,64]{3,2,1,0:T(8,128)(2,1)}, f32[8,512,64]{1,2,0:T(8,128)}, f32[8,512,64]{1,2,0:T(8,128)}, f32[8,64,320]{2,1,0:T(8,128)}...) while((s32[]{:T(128)}, ...), condition=%wide.wide.region_5.6_spmd, body=%wide.wide.region_0.5_spmd.sunk | while | flops 54078980 | bytes 11466761 | solution.py:151
  96.7 0.9 dynamic-slice_bitcast_fusion.3
  98.9 0.8 constant_dynamic-slice_fusion.23
  101.7 0.7 constant_dynamic-update-slice_fusion.44
  103.0 0.8 fusion.72
  104.8 0.9 dynamic-slice_bitcast_fusion.3
  107.0 0.8 constant_dynamic-slice_fusion.23
  109.8 0.7 constant_dynamic-update-slice_fusion.44
  110.5 0.6 bitcast_dynamic-update-slice_fusion.3
  111.2 0.8 fusion.72
  112.9 0.9 dynamic-slice_bitcast_fusion.3
  115.2 0.8 constant_dynamic-slice_fusion.23
  117.9 0.7 constant_dynamic-update-slice_fusion.44
  118.6 0.6 bitcast_dynamic-update-slice_fusion.3
  119.3 0.8 fusion.72
  121.0 0.9 dynamic-slice_bitcast_fusion.3
  123.3 0.8 constant_dynamic-slice_fusion.23
  126.0 0.7 constant_dynamic-update-slice_fusion.44
  126.7 0.6 bitcast_dynamic-update-slice_fusion.3
  127.4 0.8 fusion.72
  129.1 0.9 dynamic-slice_bitcast_fusion.3
  131.4 0.8 constant_dynamic-slice_fusion.23
  134.1 0.7 constant_dynamic-update-slice_fusion.44
  135.5 0.8 fusion.72
  137.2 0.9 dynamic-slice_bitcast_fusion.3
  139.5 0.8 constant_dynamic-slice_fusion.23
  142.2 0.7 constant_dynamic-update-slice_fusion.44
  143.0 0.6 bitcast_dynamic-update-slice_fusion.3
  143.6 0.8 fusion.72
  145.3 0.9 dynamic-slice_bitcast_fusion.3
  147.6 0.8 constant_dynamic-slice_fusion.23
  150.3 0.7 constant_dynamic-update-slice_fusion.44
  151.1 0.6 bitcast_dynamic-update-slice_fusion.3
  151.7 0.8 fusion.72
  153.5 0.9 dynamic-slice_bitcast_fusion.3
  155.7 0.8 constant_dynamic-slice_fusion.23
  158.5 0.7 constant_dynamic-update-slice_fusion.44
  159.8 0.8 fusion.72
  160.6 1.1 slice.219
  161.8 1.3 collective-permute-start.3
  163.1 2.0 rev.3
  165.6 0.8 reshape.299
  166.6 1.4 select_reduce_fusion
  168.0 0.8 copy.235
  168.8 1.1 slice.220
  169.9 1.3 collective-permute-start.2
  171.2 1.1 slice.194
  172.3 1.1 slice.192
  173.6 0.8 copy.224
  174.5 58.7 %reduce-scatter.4.cloned.1.call-done = f32[32,8]{1,0:T(8,128)} async-done(((f32[256,8]{1,0:T(8,128)}), f32[32,8]{1,0:T(8,128)}) %reduce-scatter.4.cloned.1.call-update) | async-done | bytes 1040
  233.2 0.8 copy.236
  234.0 5.2 %all_gather.3 = f32[32,32]{0,1:T(8,128)S(1)} all-gather(f32[32,8]{0,1:T(8,128)S(1)} %copy.236), channel_id=1, replica_groups=mesh['sp'=8,'tp'=4] {'tp'}, dimensions={1}, use_global_device_ids=true | all-gather | bytes 5120 | tf_op jit(solution)/shard_map/all_gather | solution.py:181
  239.2 0.7 copy.227
  239.9 0.8 copy.226
  240.8 0.8 copy.225
  (357 shorter events, 36.2 us)
Async XLA Ops:
  7.2 10.9 %copy-start = (f32[256,32]{0,1:T(8,128)S(1)}, f32[256,32]{0,1:T(8,128)}, u32[]{:S(2)}) copy-start(f32[256,32]{0,1:T(8,128)} %param.11) | copy-start | bytes 98308
  7.2 226.0 %reduce-scatter.4.cloned.1.call-start = ((), (), s32[]{:S(2)}) async-start(), calls=%async_computation.1 | async-start | bytes 147456
  8.3 87.3 %collective-permute-start = (bf16[256,512]{0,1:T(8,128)(2,1)S(1)}, bf16[256,512]{0,1:T(8,128)(2,1)S(1)}, u32[]{:S(2)}, u32[]{:S(2)}) collective-permute-start(bf16[256,512]{0,1:T(8,128)(2,1)S(1)} %copy.207), channel_id=1, source_target_pairs={{0,4},{4,8},{8,12},{12,16},{16,20},{20,24},{24,28},{1,5},{5,9},{9,... | collective-permute-start | bytes 786440 | tf_op jit(solution)/shard_map/ppermute | solution.py:20
  14.3 81.4 %collective-permute-start.1 = (bf16[256,512]{0,1:T(8,128)(2,1)S(1)}, bf16[256,512]{0,1:T(8,128)(2,1)S(1)}, u32[]{:S(2)}, u32[]{:S(2)}) collective-permute-start(bf16[256,512]{0,1:T(8,128)(2,1)S(1)} %copy.212), channel_id=1, source_target_pairs={{0,4},{4,8},{8,12},{12,16},{16,20},{20,24},{24,28},{1,5},{5,9},{9,... | collective-permute-start | bytes 786440 | tf_op jit(solution)/shard_map/ppermute | solution.py:20
  86.4 7.4 %copy-start.2 = (bf16[256,512]{1,0:T(8,128)(2,1)S(1)}, bf16[256,512]{1,0:T(8,128)(2,1)}, u32[]{:S(2)}) copy-start(bf16[256,512]{1,0:T(8,128)(2,1)} %param.7) | copy-start | bytes 786436
  86.4 7.6 %copy-start.3 = (bf16[256,512]{1,0:T(8,128)(2,1)S(1)}, bf16[256,512]{1,0:T(8,128)(2,1)}, u32[]{:S(2)}) copy-start(bf16[256,512]{1,0:T(8,128)(2,1)} %param.10) | copy-start | bytes 786436
  93.8 2.0 copy-start.4
  160.6 12.8 %copy-start.1 = (bf16[8,4,64,64]{3,2,1,0:T(8,128)(2,1)S(1)}, bf16[8,4,64,64]{3,2,1,0:T(8,128)(2,1)}, u32[]{:S(2)}) copy-start(bf16[8,4,64,64]{3,2,1,0:T(8,128)(2,1)} %get-tuple-element.146) | copy-start | bytes 786436
  161.8 78.1 %collective-permute-start.3 = (bf16[256,512]{0,1:T(8,128)(2,1)S(1)}, bf16[256,512]{0,1:T(8,128)(2,1)S(1)}, u32[]{:S(2)}, u32[]{:S(2)}) collective-permute-start(bf16[256,512]{0,1:T(8,128)(2,1)S(1)} %bitcast.268), channel_id=1, source_target_pairs={{4,0},{8,4},{12,8},{16,12},{20,16},{24,20},{28,24},{5,1},{9,5},{13... | collective-permute-start | bytes 786440 | tf_op jit(solution)/shard_map/ppermute | solution.py:20
  169.9 70.8 %collective-permute-start.2 = (bf16[256,512]{0,1:T(8,128)(2,1)S(1)}, bf16[256,512]{0,1:T(8,128)(2,1)S(1)}, u32[]{:S(2)}, u32[]{:S(2)}) collective-permute-start(bf16[256,512]{0,1:T(8,128)(2,1)S(1)} %bitcast.269), channel_id=1, source_target_pairs={{4,0},{8,4},{12,8},{16,12},{20,16},{24,20},{28,24},{5,1},{9,5},{13... | collective-permute-start | bytes 786440 | tf_op jit(solution)/shard_map/ppermute | solution.py:20
Sparse Core Ops, SparseCore 0:
  169.0 64.1 reduce-scatter.3
where the time goes:
time: 250 us; the launch traced here: 248 us
  local copies, waits for them, and re-layouts  133 us (53%)
  waiting for transfers between devices  58.7 us (23%)
  matrix products  16.8 us (7%)
  between operations  14.3 us (6%)
  starting transfers between devices  11 us (4%)
  other arithmetic  7.56 us (3%)
  blocking collectives  5.19 us (2%)
    gather x2, local copies, waits for them, and re-layouts, shards(): jnp.take(table_here, offset_index, axis=0)  74.4 us
    unnamed x2, waiting for transfers between devices  58.7 us
    dynamic_update_slice x32, local copies, waits for them, and re-layouts, shards(): lax.map(own_head, (by_heads(query_rows), by_heads(out_grad), by_heads(key...  12.7 us
    ppermute x4, starting transfers between devices, passed_along(): return lax.ppermute(block, axis, route)  10.9 us
    while x144, local copies, waits for them, and re-layouts  9.9 us
    unnamed x23, local copies, waits for them, and re-layouts  8.58 us
    dynamic_slice x32, local copies, waits for them, and re-layouts, shards(): lax.map(own_head, (by_heads(query_rows), by_heads(out_grad), by_heads(key...  8.05 us
    add x8, local copies, waits for them, and re-layouts, segment_grads(): jnp.einsum('jid,jcd->jic', query_segs, key_band, preferred_element_type=j...  7.25 us
  transfers between devices with their start and end apart: 5, of which 1 were waited for; matrix products, arithmetic and copies ran while one was open for 37% of the time, Pallas kernels for 0%

commit v1 on v0

v1 whole, which is shorter than its diff:
```python
from functools import partial
import math

import jax
import jax.numpy as jnp
from jax import lax
from jax.experimental import pallas as pl
from jax.experimental.pallas import tpu as pltpu
from jax.sharding import PartitionSpec as P

HEAD_DIM = 64
SEG = 64
LEFT = 4
CLIP = 128

LANES = 2 * HEAD_DIM
REACH = LEFT * SEG
BLK = 2 * SEG
BAND = REACH + BLK
WRAP = 3 * BLK
NEG_FILL = -1e30
LOG2E = math.log2(math.e)
MESH = pl.DeviceIdType.MESH
F32 = jnp.float32
BF16 = jnp.bfloat16

NT = (((1,), (1,)), ((), ()))
NN = (((1,), (0,)), ((), ()))
TN = (((0,), (0,)), ((), ()))


def dot(a, b, dims):
    return lax.dot_general(a, b, dims, preferred_element_type=F32)


def turned(x, amount):
    amount %= x.shape[1]
    return pltpu.roll(x, amount, 1) if amount else x


def row_turned(x, sign):
    row = lax.broadcasted_iota(jnp.int32, x.shape, 0)
    for bit in (1, 2, 4):
        x = jnp.where((row & bit) != 0, turned(x, sign * bit), x)
    return x


def build_bias(table_row, first, bias_ref, pair, lane):
    last = table_row[:, 2 * CLIP - 1 :]
    flat = jnp.broadcast_to(last, (1, BLK))
    shape = (8, BLK)
    line = jnp.concatenate([table_row[:, CLIP:], flat, table_row[:, :CLIP]], axis=1)
    base = row_turned(jnp.broadcast_to(line, (8, WRAP)), 1)
    query = lax.broadcasted_iota(jnp.int32, shape, 1)
    wall = jnp.where(first, NEG_FILL, 0.0)
    cols = pl.ds(lane * BLK, BLK)
    flat8 = jnp.broadcast_to(last, shape)
    for group in range(BAND // 8):
        row = group * 8
        if row < BLK:
            tile = flat8
        else:
            sheared = turned(base, row % BLK)
            tile = sheared[:, BLK : 2 * BLK] if row < 2 * BLK else sheared[:, :BLK]
        if row < SEG:
            tile = jnp.where(query >= SEG, NEG_FILL, tile)
        if row >= BAND - SEG:
            tile = jnp.where(query < SEG, NEG_FILL, tile)
        bias_ref[pair, 0, pl.ds(row, 8), cols] = tile + wall if row < REACH else tile
        bias_ref[pair, 1, pl.ds(row, 8), cols] = tile + wall if row < REACH - BLK else tile


def diagonals(square):
    parts = []
    for group in range(BLK // 8):
        near = square[2 * BLK + group * 8 : 2 * BLK + group * 8 + 8]
        far = square[BLK + group * 8 : BLK + group * 8 + 8]
        parts.append(jnp.concatenate([near, far, jnp.zeros_like(near)], axis=1))
    step = 8
    while len(parts) > 1:
        parts = [a + turned(b, -step) for a, b in zip(parts[::2], parts[1::2])]
        step *= 2
    sums = jnp.sum(row_turned(parts[0], -1), axis=0, keepdims=True)
    return sums, jnp.sum(square[:BLK], axis=0, keepdims=True)


def kernel(
    sp_size, tp_size,
    q_hbm, k_hbm, v_hbm, d_hbm, table_ref,
    dq_ref, dk_ref, dv_ref, dt_ref,
    q_ref, d_ref, kx, vx, bias_ref, square_ref,
    own_k, own_v, back_k, back_v, got_k, got_v,
    table_rows, pieces, piece_got, shares,
    load_sem, halo_send, halo_recv, back_send, back_recv,
    piece_send, piece_recv, share_send, share_recv,
):
    rows, width = q_hbm.shape
    pairs = width // LANES
    heads = width // HEAD_DIM
    me = lax.axis_index("sp")
    col = lax.axis_index("tp")
    has_left = me > 0
    has_right = me < sp_size - 1
    left = jnp.maximum(me - 1, 0)
    right = jnp.minimum(me + 1, sp_size - 1)

    own = pl.ds(REACH, rows)
    loads = [
        pltpu.make_async_copy(src, dst, load_sem.at[i])
        for i, (src, dst) in enumerate(
            ((k_hbm, kx.at[own]), (v_hbm, vx.at[own]), (q_hbm, q_ref), (d_hbm, d_ref))
        )
    ]
    for load in loads:
        load.start()

    barrier = pltpu.get_barrier_semaphore()
    for k in range(1, sp_size):
        pl.semaphore_signal(
            barrier, inc=1, device_id=(lax.rem(me + k, sp_size), col), device_id_type=MESH
        )
    for k in range(1, tp_size):
        pl.semaphore_signal(
            barrier, inc=1, device_id=(me, lax.rem(col + k, tp_size)), device_id_type=MESH
        )
    pl.semaphore_wait(barrier, sp_size - 1 + tp_size - 1)

    def halo_copies(p):
        cols = pl.ds(p * LANES, LANES)
        return [
            pltpu.make_async_remote_copy(
                src_ref=src.at[:, cols],
                dst_ref=dst.at[pl.ds(0, REACH), cols],
                send_sem=halo_send.at[p, i],
                recv_sem=halo_recv.at[p, i],
                device_id=(right, col),
                device_id_type=MESH,
            )
            for i, (src, dst) in enumerate(((k_hbm, kx), (v_hbm, vx)))
        ]

    def back_copies(p):
        return [
            pltpu.make_async_remote_copy(
                src_ref=src.at[p],
                dst_ref=dst.at[p],
                send_sem=back_send.at[p, i],
                recv_sem=back_recv.at[p, i],
                device_id=(left, col),
                device_id_type=MESH,
            )
            for i, (src, dst) in enumerate(((back_k, got_k), (back_v, got_v)))
        ]

    @pl.when(has_right)
    def _():
        for p in range(pairs):
            for copy in halo_copies(p):
                copy.start()

    @pl.when(jnp.logical_not(has_left))
    def _():
        kx[0:REACH, :] = jnp.zeros((REACH, width), BF16)
        vx[0:REACH, :] = jnp.zeros((REACH, width), BF16)

    table_rows[...] = jnp.transpose(table_ref[...]) * LOG2E
    for h in range(heads):
        row = table_rows[pl.ds(col * heads + h, 1), :]
        build_bias(row, jnp.logical_not(has_left), bias_ref, h // 2, h % 2)

    for load in loads:
        load.wait()

    low = lax.broadcasted_iota(jnp.int32, (BLK, LANES), 1) < HEAD_DIM
    scale = HEAD_DIM ** -0.5
    sums, tops = [], []

    def split(x):
        zero = jnp.zeros_like(x)
        return jnp.concatenate([jnp.where(low, x, zero), jnp.where(low, zero, x)], axis=0)

    for p in range(pairs):
        cols = pl.ds(p * LANES, LANES)

        @pl.when(has_left)
        def _():
            for copy in halo_copies(p):
                copy.wait_recv()

        grads = []
        for half in range(2):
            keys = pl.ds(half * BLK, BAND)
            mine = pl.ds(half * BLK, BLK)
            k_blk = kx[keys, cols]
            v_blk = vx[keys, cols]
            qq = split(q_ref[mine, cols] * jnp.asarray(scale, BF16))
            dd = split(d_ref[mine, cols])
            scores = dot(k_blk, qq, NT) * LOG2E + bias_ref[p, half]
            dprobs = dot(v_blk, dd, NT)
            peak = jnp.max(scores, axis=0, keepdims=True)
            grown = jnp.exp2(scores - peak)
            inverse = 1.0 / jnp.sum(grown, axis=0, keepdims=True)
            probs = grown * inverse
            inner = jnp.sum(probs * dprobs, axis=0, keepdims=True)
            dscores = probs * (dprobs - inner)
            if half == 0:
                square_ref[...] = dscores
            else:
                square_ref[...] += dscores
            ds_half = dscores.astype(BF16)
            grads.append((dot(ds_half, qq, NN), dot(probs.astype(BF16), dd, NN)))
            flat = dot(k_blk, ds_half, TN)
            both = jnp.concatenate([flat[:HEAD_DIM, :BLK], flat[HEAD_DIM:, BLK:]], axis=0)
            dq_ref[mine, cols] = (jnp.transpose(both) * scale).astype(BF16)
        for i, (back, mine_ref) in enumerate(((back_k, own_k), (back_v, own_v))):
            a, b = grads[0][i], grads[1][i]
            back[p, 0:BLK, :] = a[:BLK].astype(BF16)
            back[p, BLK:REACH, :] = (a[BLK:REACH] + b[: REACH - BLK]).astype(BF16)
            mine_ref[p, 0:BLK, :] = a[REACH:] + b[REACH - BLK : REACH]
            mine_ref[p, BLK:rows, :] = b[REACH:]

        @pl.when(has_left)
        def _():
            for copy in back_copies(p):
                copy.start()

        for lane in range(2):
            s, t = diagonals(square_ref[:, lane * BLK : (lane + 1) * BLK])
            sums.append(s)
            tops.append(t)

    y = jnp.concatenate(sums, axis=0)
    beyond = jnp.sum(
        y[:, BLK : 2 * BLK] + jnp.concatenate(tops, axis=0), axis=1, keepdims=True
    )
    spot = lax.broadcasted_iota(jnp.int32, (heads, BLK), 1)
    upper = y[:, :BLK] + jnp.where(spot == BLK - 1, beyond, 0.0)
    grad_rows = jnp.concatenate([y[:, 2 * BLK :], upper], axis=1)
    part = 2 * CLIP // sp_size
    for s in range(sp_size):
        pieces[s] = turned(grad_rows, -part * s)[:, :BLK]

    def piece_copy(k):
        target = lax.rem(me + k, sp_size)
        return pltpu.make_async_remote_copy(
            src_ref=pieces.at[target],
            dst_ref=piece_got.at[k - 1],
            send_sem=piece_send.at[k - 1],
            recv_sem=piece_recv.at[k - 1],
            device_id=(target, col),
            device_id_type=MESH,
        )

    def share_copy(k):
        return pltpu.make_async_remote_copy(
            src_ref=shares.at[col],
            dst_ref=shares.at[col],
            send_sem=share_send.at[k - 1],
            recv_sem=share_recv.at[k - 1],
            device_id=(me, lax.rem(col + k, tp_size)),
            device_id_type=MESH,
        )

    def share_arrival(k):
        source = lax.rem(col + tp_size - k, tp_size)
        return pltpu.make_async_remote_copy(
            src_ref=shares.at[source],
            dst_ref=shares.at[source],
            send_sem=share_send.at[k - 1],
            recv_sem=share_recv.at[k - 1],
            device_id=(me, source),
            device_id_type=MESH,
        )

    for k in range(1, sp_size):
        piece_copy(k).start()

    def finish(p):
        cols = pl.ds(p * LANES, LANES)

        @pl.when(has_right)
        def _():
            for copy in back_copies(p):
                copy.wait_recv()
            dk_ref[:, cols] = (own_k[p] + got_k[p].astype(F32)).astype(BF16)
            dv_ref[:, cols] = (own_v[p] + got_v[p].astype(F32)).astype(BF16)

        @pl.when(jnp.logical_not(has_right))
        def _():
            dk_ref[:, cols] = own_k[p].astype(BF16)
            dv_ref[:, cols] = own_v[p].astype(BF16)

    total = pieces[me]
    for k in range(1, sp_size):
        piece_copy(k).wait_recv()
        total = total + piece_got[k - 1]
    shares[col] = total
    for k in range(1, tp_size):
        share_copy(k).start()
    for p in range(pairs):
        finish(p)
    for k in range(1, tp_size):
        share_arrival(k).wait_recv()
    stacked = jnp.concatenate([shares[t] for t in range(tp_size)], axis=0)
    dt_ref[...] = jnp.transpose(stacked)[:part]

    for k in range(1, sp_size):
        piece_copy(k).wait_send()
    for k in range(1, tp_size):
        share_copy(k).wait_send()

    @pl.when(has_right)
    def _():
        for p in range(pairs):
            for copy in halo_copies(p):
                copy.wait_send()

    @pl.when(has_left)
    def _():
        for p in range(pairs):
            for copy in back_copies(p):
                copy.wait_send()


def shards(sp_size, tp_size, query_rows, key_rows, value_rows, out_grad, rel_bias):
    rows, width = query_rows.shape
    pairs = width // LANES
    heads = width // HEAD_DIM
    part = 2 * CLIP // sp_size
    assert rows == REACH and REACH == 2 * BLK and CLIP == BLK
    like = jax.ShapeDtypeStruct((rows, width), BF16)
    dma = pltpu.SemaphoreType.DMA
    return pl.pallas_call(
        partial(kernel, sp_size, tp_size),
        out_shape=(like, like, like, jax.ShapeDtypeStruct((part, heads * tp_size), F32)),
        in_specs=[pl.BlockSpec(memory_space=pl.ANY)] * 4
        + [pl.BlockSpec(memory_space=pltpu.VMEM)],
        out_specs=tuple([pl.BlockSpec(memory_space=pltpu.VMEM)] * 4),
        scratch_shapes=[
            pltpu.VMEM((rows, width), BF16),
            pltpu.VMEM((rows, width), BF16),
            pltpu.VMEM((REACH + rows, width), BF16),
            pltpu.VMEM((REACH + rows, width), BF16),
            pltpu.VMEM((pairs, 2, BAND, 2 * BLK), F32),
            pltpu.VMEM((BAND, 2 * BLK), F32),
            pltpu.VMEM((pairs, rows, LANES), F32),
            pltpu.VMEM((pairs, rows, LANES), F32),
            pltpu.VMEM((pairs, REACH, LANES), BF16),
            pltpu.VMEM((pairs, REACH, LANES), BF16),
            pltpu.VMEM((pairs, REACH, LANES), BF16),
            pltpu.VMEM((pairs, REACH, LANES), BF16),
            pltpu.VMEM(rel_bias.shape[::-1], F32),
            pltpu.VMEM((sp_size, heads, BLK), F32),
            pltpu.VMEM((sp_size - 1, heads, BLK), F32),
            pltpu.VMEM((tp_size, heads, BLK), F32),
            dma((4,)),
            dma((pairs, 2)),
            dma((pairs, 2)),
            dma((pairs, 2)),
            dma((pairs, 2)),
            dma((sp_size - 1,)),
            dma((sp_size - 1,)),
            dma((tp_size - 1,)),
            dma((tp_size - 1,)),
        ],
        compiler_params=pltpu.CompilerParams(
            collective_id=0, has_side_effects=True, vmem_limit_bytes=48 * 1024 * 1024
        ),
    )(query_rows, key_rows, value_rows, out_grad, rel_bias)


def solution(mesh):
    return jax.shard_map(
        partial(shards, mesh.shape["sp"], mesh.shape["tp"]),
        mesh=mesh,
        in_specs=(P("sp", "tp"), P("sp", "tp"), P("sp", "tp"), P("sp", "tp"), P()),
        out_specs=(P("sp", "tp"), P("sp", "tp"), P("sp", "tp"), P("sp", None)),
        check_vma=False,
    )
```

time: 250 us -> 48.8 us (0.20)
  local copies, waits for them, and re-layouts: 133 us -> 7.36 us
  waiting for transfers between devices: 58.7 us -> 0 us
  Pallas kernels: 0 us -> 40.5 us
  matrix products: 16.8 us -> 0 us
  between operations: 14.3 us -> 0.65 us
  starting transfers between devices: 11 us -> 0 us
  other arithmetic: 7.56 us -> 0 us
  blocking collectives: 5.19 us -> 0 us
    gather x2 -> x0, local copies, waits for them, and re-layouts: 74.4 us -> none  [shards(): jnp.take(table_here, offset_index, axis=0)]
    unnamed x2 -> x0, waiting for transfers between devices: 58.7 us -> none
    pallas_call x0 -> x1, Pallas kernels: none -> 40.5 us  [shards(): pl.pallas_call(partial(kernel, sp_size, tp_size), out_shape=(like, like,...]
    dot_general x40 -> x0, matrix products: 16.8 us -> none  [the longest x8 6.6 us: segment_grads(): jnp.einsum('jic,jcd->jid', dscore_half, key_band, preferred_element_type=...]
    dynamic_update_slice x32 -> x0, local copies, waits for them, and re-layouts: 12.7 us -> none  [shards(): lax.map(own_head, (by_heads(query_rows), by_heads(out_grad), by_heads(key...]
    ppermute x4 -> x0, starting transfers between devices: 10.9 us -> none  [passed_along(): return lax.ppermute(block, axis, route)]
    while x144 -> x0, local copies, waits for them, and re-layouts: 9.9 us -> none
    dynamic_slice x33 -> x0, local copies, waits for them, and re-layouts: 8.06 us -> none  [the longest x32 8.05 us: shards(): lax.map(own_head, (by_heads(query_rows), by_heads(out_grad), by_heads(key...]
  transfers between devices with their start and end apart: 5 -> 0, of which waited for: 1 -> 0; matrix products, arithmetic and copies ran while one was open for 37% -> 0% of each run, Pallas kernels for 0% -> 0%
where the time goes in v1:
time: 48.8 us; the launch traced here: 48.5 us
  Pallas kernels  40.5 us (83%)
  local copies, waits for them, and re-layouts  7.36 us (15%)
  between operations  0.65 us (1%)
    pallas_call x1, Pallas kernels, shards(): pl.pallas_call(partial(kernel, sp_size, tp_size), out_shape=(like, like,...  40.5 us
    unnamed x13, local copies, waits for them, and re-layouts  7.36 us

profile of v1, /device:TPU:0, one launch (start us, length us, event | category | flops | bytes accessed | tf_op | source)
XLA Modules:
  0.0 48.5 jit_solution(7329344700986508458)
XLA Ops:
  0.6 0.9 %copy.9.table_ref = f32[256,32]{1,0:T(8,128)S(1)} copy(f32[256,32]{0,1:T(8,128)} %param.9) | data formatting | bytes 65536 | tf_op args[4]
  1.5 0.0 copy-start
  1.5 0.9 %copy-done = bf16[256,512]{1,0:T(8,128)(2,1)S(1)} copy-done((bf16[256,512]{1,0:T(8,128)(2,1)S(1)}, bf16[256,512]{1,0:T(8,128)(2,1)}, u32[]{:S(2)}) %copy-start) | copy-done | bytes 262168
  2.4 0.0 copy-start.1
  2.4 0.9 %copy-done.1 = bf16[256,512]{1,0:T(8,128)(2,1)S(1)} copy-done((bf16[256,512]{1,0:T(8,128)(2,1)S(1)}, bf16[256,512]{1,0:T(8,128)(2,1)}, u32[]{:S(2)}) %copy-start.1) | copy-done | bytes 262168
  3.4 0.0 copy-start.2
  3.4 0.9 %copy-done.2 = bf16[256,512]{1,0:T(8,128)(2,1)S(1)} copy-done((bf16[256,512]{1,0:T(8,128)(2,1)S(1)}, bf16[256,512]{1,0:T(8,128)(2,1)}, u32[]{:S(2)}) %copy-start.2) | copy-done | bytes 262168
  4.3 0.0 copy-start.3
  4.3 0.9 %copy-done.3 = bf16[256,512]{1,0:T(8,128)(2,1)S(1)} copy-done((bf16[256,512]{1,0:T(8,128)(2,1)S(1)}, bf16[256,512]{1,0:T(8,128)(2,1)}, u32[]{:S(2)}) %copy-start.3) | copy-done | bytes 262168
  5.3 40.5 %shard_map.84 = (bf16[256,512]{1,0:T(8,128)(2,1)S(1)}, bf16[256,512]{1,0:T(8,128)(2,1)S(1)}, bf16[256,512]{1,0:T(8,128)(2,1)S(1)}, f32[32,32]{1,0:T(8,128)S(1)}) custom-call(bf16[256,512]{1,0:T(8,128)(2,1)S(1)} %copy-done, bf16[256,512]{1,0:T(8,128)(2,1)S(1)} %copy-done.1, bf16[256,512]{1,0:T(8,128)(2,1)S(1)} %copy-done.2, bf16[256,512]{1,0:T(8,128)(2,1)S(1)} %copy-done.3, ...), custom_call_target="tpu_custom_call" | custom-call | tf_op jit(solution)/shard_map/pallas_call | solution.py:333
  45.8 0.7 %copy.14 = bf16[256,512]{1,0:T(8,128)(2,1)} copy(bf16[256,512]{1,0:T(8,128)(2,1)S(1)} %get-tuple-element.8) | data formatting | bytes 524288
  46.5 0.7 %copy.15 = bf16[256,512]{1,0:T(8,128)(2,1)} copy(bf16[256,512]{1,0:T(8,128)(2,1)S(1)} %get-tuple-element.9) | data formatting | bytes 524288
  47.2 0.7 %copy.16 = bf16[256,512]{1,0:T(8,128)(2,1)} copy(bf16[256,512]{1,0:T(8,128)(2,1)S(1)} %get-tuple-element.10) | data formatting | bytes 524288
  47.9 0.6 %copy.17 = f32[32,32]{1,0:T(8,128)} copy(f32[32,32]{1,0:T(8,128)S(1)} %get-tuple-element.11) | data formatting | bytes 8192
Async XLA Ops:
  1.5 1.0 %copy-start = (bf16[256,512]{1,0:T(8,128)(2,1)S(1)}, bf16[256,512]{1,0:T(8,128)(2,1)}, u32[]{:S(2)}) copy-start(bf16[256,512]{1,0:T(8,128)(2,1)} %q_hbm.1) | copy-start | bytes 786436
  2.4 0.9 %copy-start.1 = (bf16[256,512]{1,0:T(8,128)(2,1)S(1)}, bf16[256,512]{1,0:T(8,128)(2,1)}, u32[]{:S(2)}) copy-start(bf16[256,512]{1,0:T(8,128)(2,1)} %k_hbm.1) | copy-start | bytes 786436
  3.4 0.9 %copy-start.2 = (bf16[256,512]{1,0:T(8,128)(2,1)S(1)}, bf16[256,512]{1,0:T(8,128)(2,1)}, u32[]{:S(2)}) copy-start(bf16[256,512]{1,0:T(8,128)(2,1)} %v_hbm.1) | copy-start | bytes 786436
  4.3 0.9 %copy-start.3 = (bf16[256,512]{1,0:T(8,128)(2,1)S(1)}, bf16[256,512]{1,0:T(8,128)(2,1)}, u32[]{:S(2)}) copy-start(bf16[256,512]{1,0:T(8,128)(2,1)} %d_hbm.1) | copy-start | bytes 786436

commit v2 on v1

--- a/solution.py
+++ b/solution.py
@@ -86,7 +86,7 @@
 
 def kernel(
     sp_size, tp_size,
-    q_hbm, k_hbm, v_hbm, d_hbm, table_ref,
+    q_hbm, k_hbm, v_hbm, d_hbm, table_hbm,
     dq_ref, dk_ref, dv_ref, dt_ref,
     q_ref, d_ref, kx, vx, bias_ref, square_ref,
     own_k, own_v, back_k, back_v, got_k, got_v,
@@ -108,7 +108,13 @@
     loads = [
         pltpu.make_async_copy(src, dst, load_sem.at[i])
         for i, (src, dst) in enumerate(
-            ((k_hbm, kx.at[own]), (v_hbm, vx.at[own]), (q_hbm, q_ref), (d_hbm, d_ref))
+            (
+                (k_hbm, kx.at[own]),
+                (v_hbm, vx.at[own]),
+                (q_hbm, q_ref),
+                (d_hbm, d_ref),
+                (table_hbm, table_rows),
+            )
         )
     ]
     for load in loads:
@@ -152,6 +158,12 @@
             for i, (src, dst) in enumerate(((back_k, got_k), (back_v, got_v)))
         ]
 
+    def send_back(p):
+        @pl.when(has_left)
+        def _():
+            for copy in back_copies(p):
+                copy.start()
+
     @pl.when(has_right)
     def _():
         for p in range(pairs):
@@ -163,17 +175,18 @@
         kx[0:REACH, :] = jnp.zeros((REACH, width), BF16)
         vx[0:REACH, :] = jnp.zeros((REACH, width), BF16)
 
-    table_rows[...] = jnp.transpose(table_ref[...]) * LOG2E
+    loads[4].wait()
     for h in range(heads):
-        row = table_rows[pl.ds(col * heads + h, 1), :]
+        row = table_rows[pl.ds(col * heads + h, 1), :] * LOG2E
         build_bias(row, jnp.logical_not(has_left), bias_ref, h // 2, h % 2)
 
-    for load in loads:
+    for load in loads[:4]:
         load.wait()
 
     low = lax.broadcasted_iota(jnp.int32, (BLK, LANES), 1) < HEAD_DIM
     scale = HEAD_DIM ** -0.5
     sums, tops = [], []
+    held = pairs
 
     def split(x):
         zero = jnp.zeros_like(x)
@@ -219,11 +232,8 @@
             mine_ref[p, 0:BLK, :] = a[REACH:] + b[REACH - BLK : REACH]
             mine_ref[p, BLK:rows, :] = b[REACH:]
 
-        @pl.when(has_left)
-        def _():
-            for copy in back_copies(p):
-                copy.start()
-
+        if p < pairs - held:
+            send_back(p)
         for lane in range(2):
             s, t = diagonals(square_ref[:, lane * BLK : (lane + 1) * BLK])
             sums.append(s)
@@ -274,6 +284,8 @@
 
     for k in range(1, sp_size):
         piece_copy(k).start()
+    for p in range(pairs - held, pairs):
+        send_back(p)
 
     def finish(p):
         cols = pl.ds(p * LANES, LANES)
@@ -330,11 +342,11 @@
     assert rows == REACH and REACH == 2 * BLK and CLIP == BLK
     like = jax.ShapeDtypeStruct((rows, width), BF16)
     dma = pltpu.SemaphoreType.DMA
-    return pl.pallas_call(
+    shapes = (like, like, like, jax.ShapeDtypeStruct((part, heads * tp_size), F32))
+    results = pl.pallas_call(
         partial(kernel, sp_size, tp_size),
-        out_shape=(like, like, like, jax.ShapeDtypeStruct((part, heads * tp_size), F32)),
-        in_specs=[pl.BlockSpec(memory_space=pl.ANY)] * 4
-        + [pl.BlockSpec(memory_space=pltpu.VMEM)],
+        out_shape=shapes,
+        in_specs=[pl.BlockSpec(memory_space=pltpu.HBM)] * 5,
         out_specs=tuple([pl.BlockSpec(memory_space=pltpu.VMEM)] * 4),
         scratch_shapes=[
             pltpu.VMEM((rows, width), BF16),
@@ -353,7 +365,7 @@
             pltpu.VMEM((sp_size, heads, BLK), F32),
             pltpu.VMEM((sp_size - 1, heads, BLK), F32),
             pltpu.VMEM((tp_size, heads, BLK), F32),
-            dma((4,)),
+            dma((5,)),
             dma((pairs, 2)),
             dma((pairs, 2)),
             dma((pairs, 2)),
@@ -366,7 +378,24 @@
         compiler_params=pltpu.CompilerParams(
             collective_id=0, has_side_effects=True, vmem_limit_bytes=48 * 1024 * 1024
         ),
-    )(query_rows, key_rows, value_rows, out_grad, rel_bias)
+    )(*[pltpu.with_memory_space_constraint(x, pltpu.HBM) for x in (query_rows, key_rows, value_rows, out_grad, jnp.transpose(rel_bias))])
+    return pl.pallas_call(
+        write_out,
+        out_shape=shapes,
+        in_specs=[pl.BlockSpec(memory_space=pl.ANY)] * 4,
+        out_specs=tuple([pl.BlockSpec(memory_space=pltpu.HBM)] * 4),
+        scratch_shapes=[dma((4,))],
+        compiler_params=pltpu.CompilerParams(vmem_limit_bytes=1024 * 1024),
+    )(*results)
+
+
+def write_out(*refs):
+    sem = refs[-1]
+    copies = [pltpu.make_async_copy(refs[i], refs[4 + i], sem.at[i]) for i in range(4)]
+    for copy in copies:
+        copy.start()
+    for copy in copies:
+        copy.wait()
 
 
 def solution(mesh):

time: 48.8 us -> 35.3 us (0.72)
  local copies, waits for them, and re-layouts: 7.36 us -> 0 us
  Pallas kernels: 40.5 us -> 34.5 us
    unnamed x13 -> x0, local copies, waits for them, and re-layouts: 7.36 us -> none
    pallas_call x1 -> x2, Pallas kernels: 40.5 us -> 34.5 us  [the longest x1 33.6 us: shards(): pl.pallas_call(partial(kernel, sp_size, tp_size), out_shape=shapes, in_sp...]
where the time goes in v2:
time: 35.3 us; the launch traced here: 35.2 us
  Pallas kernels  34.5 us (98%)
  between operations  0.64 us (2%)
    pallas_call x1, Pallas kernels, shards(): pl.pallas_call(partial(kernel, sp_size, tp_size), out_shape=shapes, in_sp...  33.6 us
    pallas_call x1, Pallas kernels, shards(): pl.pallas_call(write_out, out_shape=shapes, in_specs=[pl.BlockSpec(memory...  0.91 us

profile of v2, /device:TPU:0, one launch (start us, length us, event | category | flops | bytes accessed | tf_op | source)
XLA Modules:
  0.0 35.2 jit_solution(783898077177377807)
XLA Ops:
  0.6 33.6 %shard_map.84 = (bf16[256,512]{1,0:T(8,128)(2,1)S(1)}, bf16[256,512]{1,0:T(8,128)(2,1)S(1)}, bf16[256,512]{1,0:T(8,128)(2,1)S(1)}, f32[32,32]{1,0:T(8,128)S(1)}) custom-call(bf16[256,512]{1,0:T(8,128)(2,1)} %q_hbm.1, bf16[256,512]{1,0:T(8,128)(2,1)} %k_hbm.1, bf16[256,512]{1,0:T(8,128)(2,1)} %v_hbm.1, bf16[256,512]{1,0:T(8,128)(2,1)} %d_hbm.1, f32[32,256]{1,0:T(8,128)} %bitcast.1), custom_call_target="tpu_custom_call" | custom-call | tf_op jit(solution)/shard_map/pallas_call | solution.py:346
  34.3 0.9 %shard_map.85 = (bf16[256,512]{1,0:T(8,128)(2,1)}, bf16[256,512]{1,0:T(8,128)(2,1)}, bf16[256,512]{1,0:T(8,128)(2,1)}, f32[32,32]{1,0:T(8,128)}) custom-call(bf16[256,512]{1,0:T(8,128)(2,1)S(1)} %get-tuple-element.8.refs_0_, bf16[256,512]{1,0:T(8,128)(2,1)S(1)} %get-tuple-element.9.refs_1_, bf16[256,512]{1,0:T(8,128)(2,1)S(1)} %get-tuple-element.10.refs_2_, ...), custom_call_target="tpu_custom_call" | custom-call | tf_op jit(solution)/shard_map/pallas_call | solution.py:382

commit v3 on v2

--- a/solution.py
+++ b/solution.py
@@ -45,14 +45,13 @@
     return x
 
 
-def build_bias(table_row, first, bias_ref, pair, lane):
+def build_bias(table_row, bias_ref, pair, lane):
     last = table_row[:, 2 * CLIP - 1 :]
     flat = jnp.broadcast_to(last, (1, BLK))
     shape = (8, BLK)
     line = jnp.concatenate([table_row[:, CLIP:], flat, table_row[:, :CLIP]], axis=1)
     base = row_turned(jnp.broadcast_to(line, (8, WRAP)), 1)
     query = lax.broadcasted_iota(jnp.int32, shape, 1)
-    wall = jnp.where(first, NEG_FILL, 0.0)
     cols = pl.ds(lane * BLK, BLK)
     flat8 = jnp.broadcast_to(last, shape)
     for group in range(BAND // 8):
@@ -66,8 +65,7 @@
             tile = jnp.where(query >= SEG, NEG_FILL, tile)
         if row >= BAND - SEG:
             tile = jnp.where(query < SEG, NEG_FILL, tile)
-        bias_ref[pair, 0, pl.ds(row, 8), cols] = tile + wall if row < REACH else tile
-        bias_ref[pair, 1, pl.ds(row, 8), cols] = tile + wall if row < REACH - BLK else tile
+        bias_ref[pair, pl.ds(row, 8), cols] = tile
 
 
 def diagonals(square):
@@ -88,10 +86,11 @@
     sp_size, tp_size,
     q_hbm, k_hbm, v_hbm, d_hbm, table_hbm,
     dq_ref, dk_ref, dv_ref, dt_ref,
-    q_ref, d_ref, kx, vx, bias_ref, square_ref,
-    own_k, own_v, back_k, back_v, got_k, got_v,
+    qx, dx, k_ref, v_ref, bias_ref, square_ref, grown_ref, dprob_ref,
+    own_k, own_v, own_q, back_q, got_q,
+    local_stats, right_stats, halo_stats, left_stats,
     table_rows, pieces, piece_got, shares,
-    load_sem, halo_send, halo_recv, back_send, back_recv,
+    load_sem, seq_send, seq_recv, ls_send, ls_recv, hs_send, hs_recv, back_send, back_recv,
     piece_send, piece_recv, share_send, share_recv,
 ):
     rows, width = q_hbm.shape
@@ -104,15 +103,15 @@
     left = jnp.maximum(me - 1, 0)
     right = jnp.minimum(me + 1, sp_size - 1)
 
-    own = pl.ds(REACH, rows)
+    own = pl.ds(0, rows)
     loads = [
         pltpu.make_async_copy(src, dst, load_sem.at[i])
         for i, (src, dst) in enumerate(
             (
-                (k_hbm, kx.at[own]),
-                (v_hbm, vx.at[own]),
-                (q_hbm, q_ref),
-                (d_hbm, d_ref),
+                (k_hbm, k_ref),
+                (v_hbm, v_ref),
+                (q_hbm, qx.at[own]),
+                (d_hbm, dx.at[own]),
                 (table_hbm, table_rows),
             )
         )
@@ -131,54 +130,58 @@
         )
     pl.semaphore_wait(barrier, sp_size - 1 + tp_size - 1)
 
-    def halo_copies(p):
+    def remote(src, dst, send, recv, target):
+        return pltpu.make_async_remote_copy(
+            src_ref=src,
+            dst_ref=dst,
+            send_sem=send,
+            recv_sem=recv,
+            device_id=(target, col),
+            device_id_type=MESH,
+        )
+
+    def seq_copies(p):
         cols = pl.ds(p * LANES, LANES)
         return [
-            pltpu.make_async_remote_copy(
-                src_ref=src.at[:, cols],
-                dst_ref=dst.at[pl.ds(0, REACH), cols],
-                send_sem=halo_send.at[p, i],
-                recv_sem=halo_recv.at[p, i],
-                device_id=(right, col),
-                device_id_type=MESH,
+            remote(
+                src.at[:, cols],
+                dst.at[pl.ds(rows, rows), cols],
+                seq_send.at[p, i],
+                seq_recv.at[p, i],
+                left,
             )
-            for i, (src, dst) in enumerate(((k_hbm, kx), (v_hbm, vx)))
+            for i, (src, dst) in enumerate(((q_hbm, qx), (d_hbm, dx)))
         ]
 
-    def back_copies(p):
-        return [
-            pltpu.make_async_remote_copy(
-                src_ref=src.at[p],
-                dst_ref=dst.at[p],
-                send_sem=back_send.at[p, i],
-                recv_sem=back_recv.at[p, i],
-                device_id=(left, col),
-                device_id_type=MESH,
-            )
-            for i, (src, dst) in enumerate(((back_k, got_k), (back_v, got_v)))
-        ]
-
-    def send_back(p):
-        @pl.when(has_left)
-        def _():
-            for copy in back_copies(p):
+    def local_copy():
+        return remote(local_stats, right_stats, ls_send, ls_recv, left)
+
+    def halo_copy(p):
+        return remote(halo_stats.at[p], left_stats.at[p], hs_send.at[p], hs_recv.at[p], right)
+
+    def back_copy(p):
+        return remote(back_q.at[p], got_q.at[p], back_send.at[p], back_recv.at[p], right)
+
+    early = (pairs + 1) // 2
+
+    @pl.when(has_left)
+    def _():
+        for p in range(early):
+            for copy in seq_copies(p):
                 copy.start()
 
-    @pl.when(has_right)
-    def _():
-        for p in range(pairs):
-            for copy in halo_copies(p):
-                copy.start()
+    local_stats[...] = jnp.zeros(local_stats.shape, F32)
+    halo_stats[...] = jnp.zeros(halo_stats.shape, F32)
 
     @pl.when(jnp.logical_not(has_left))
     def _():
-        kx[0:REACH, :] = jnp.zeros((REACH, width), BF16)
-        vx[0:REACH, :] = jnp.zeros((REACH, width), BF16)
+        spot = lax.broadcasted_iota(jnp.int32, left_stats.shape, 1)
+        left_stats[...] = jnp.where((spot == 0) | (spot == 3), NEG_FILL, 0.0)
 
     loads[4].wait()
     for h in range(heads):
         row = table_rows[pl.ds(col * heads + h, 1), :] * LOG2E
-        build_bias(row, jnp.logical_not(has_left), bias_ref, h // 2, h % 2)
+        build_bias(row, bias_ref, h // 2, h % 2)
 
     for load in loads[:4]:
         load.wait()
@@ -186,58 +189,139 @@
     low = lax.broadcasted_iota(jnp.int32, (BLK, LANES), 1) < HEAD_DIM
     scale = HEAD_DIM ** -0.5
     sums, tops = [], []
-    held = pairs
 
     def split(x):
         zero = jnp.zeros_like(x)
         return jnp.concatenate([jnp.where(low, x, zero), jnp.where(low, zero, x)], axis=0)
 
+    def tile(p, half, halo):
+        cols = pl.ds(p * LANES, LANES)
+        mine = pl.ds(half * BLK + (rows if halo else 0), BLK)
+        start, size, row = (
+            (half * BLK, REACH - half * BLK, 0)
+            if halo
+            else (0, (half + 1) * BLK, REACH - half * BLK)
+        )
+        keys = pl.ds(start, size)
+        qq = split(qx[mine, cols] * jnp.asarray(scale, BF16))
+        dd = split(dx[mine, cols])
+        return k_ref[keys, cols], v_ref[keys, cols], qq, dd, pl.ds(row, size)
+
+    def partial_softmax(p, half, halo, stats):
+        k_blk, v_blk, qq, dd, band = tile(p, half, halo)
+        scores = dot(k_blk, qq, NT) * LOG2E + bias_ref[p, band]
+        dprobs = dot(v_blk, dd, NT)
+        peak = jnp.max(scores, axis=0, keepdims=True)
+        grown = jnp.exp2(scores - peak)
+        three = (
+            peak,
+            jnp.sum(grown, axis=0, keepdims=True),
+            jnp.sum(grown * dprobs, axis=0, keepdims=True),
+        )
+        for i, value in enumerate(three):
+            stats[p, pl.ds(half * 3 + i, 1), :] = value
+        return grown, dprobs
+
+    def tile_grads(p, half, halo, grown, dprobs, stats, others):
+        k_blk, v_blk, qq, dd, band = tile(p, half, halo)
+        m1, l1, i1 = (stats[p, pl.ds(half * 3 + i, 1), :] for i in range(3))
+        m2, l2, i2 = (others[p, pl.ds(half * 3 + i, 1), :] for i in range(3))
+        peak = jnp.maximum(m1, m2)
+        a1, a2 = jnp.exp2(m1 - peak), jnp.exp2(m2 - peak)
+        inverse = 1.0 / (l1 * a1 + l2 * a2)
+        inner = (i1 * a1 + i2 * a2) * inverse
+        probs = grown * (a1 * inverse)
+        dscores = probs * (dprobs - inner)
+        ds_half = dscores.astype(BF16)
+        flat = dot(k_blk, ds_half, TN)
+        both = jnp.concatenate([flat[:HEAD_DIM, :BLK], flat[HEAD_DIM:, BLK:]], axis=0)
+        return (
+            dscores,
+            dot(ds_half, qq, NN),
+            dot(probs.astype(BF16), dd, NN),
+            jnp.transpose(both) * scale,
+        )
+
+    places = (pl.ds(0, BLK), pl.ds(BLK, 2 * BLK))
     for p in range(pairs):
+        for half in range(2):
+            grown, dprobs = partial_softmax(p, half, False, local_stats)
+            grown_ref[p, places[half], :] = grown
+            dprob_ref[p, places[half], :] = dprobs
+
+    @pl.when(has_left)
+    def _():
+        local_copy().start()
+        for p in range(early, pairs):
+            for copy in seq_copies(p):
+                copy.start()
+
+    def halo(p):
+        @pl.when(has_right)
+        def _():
+            for copy in seq_copies(p):
+                copy.wait_recv()
+            kept = [partial_softmax(p, half, True, halo_stats) for half in range(2)]
+            halo_copy(p).start()
+            if p == 0:
+                local_copy().wait_recv()
+            (s0, k0, v0, q0), (s1, k1, v1, q1) = (
+                tile_grads(p, half, True, *kept[half], halo_stats, right_stats)
+                for half in range(2)
+            )
+            for ref, a, b in ((own_k, k0, k1), (own_v, v0, v1)):
+                ref[p, :BLK, :] = a[:BLK]
+                ref[p, BLK:, :] = a[BLK:] + b
+            back_q[p, :BLK, :] = q0.astype(BF16)
+            back_q[p, BLK:, :] = q1.astype(BF16)
+            square_ref[p, :BLK, :] = s0[:BLK] + s1
+            square_ref[p, BLK:REACH, :] = s0[BLK:]
+
+        @pl.when(jnp.logical_not(has_right))
+        def _():
+            own_k[p] = jnp.zeros((rows, LANES), F32)
+            own_v[p] = jnp.zeros((rows, LANES), F32)
+            square_ref[p, :REACH, :] = jnp.zeros((REACH, 2 * BLK), F32)
+
+    def local(p):
         cols = pl.ds(p * LANES, LANES)
 
         @pl.when(has_left)
         def _():
-            for copy in halo_copies(p):
-                copy.wait_recv()
-
-        grads = []
-        for half in range(2):
-            keys = pl.ds(half * BLK, BAND)
-            mine = pl.ds(half * BLK, BLK)
-            k_blk = kx[keys, cols]
-            v_blk = vx[keys, cols]
-            qq = split(q_ref[mine, cols] * jnp.asarray(scale, BF16))
-            dd = split(d_ref[mine, cols])
-            scores = dot(k_blk, qq, NT) * LOG2E + bias_ref[p, half]
-            dprobs = dot(v_blk, dd, NT)
-            peak = jnp.max(scores, axis=0, keepdims=True)
-            grown = jnp.exp2(scores - peak)
-            inverse = 1.0 / jnp.sum(grown, axis=0, keepdims=True)
-            probs = grown * inverse
-            inner = jnp.sum(probs * dprobs, axis=0, keepdims=True)
-            dscores = probs * (dprobs - inner)
-            if half == 0:
-                square_ref[...] = dscores
-            else:
-                square_ref[...] += dscores
-            ds_half = dscores.astype(BF16)
-            grads.append((dot(ds_half, qq, NN), dot(probs.astype(BF16), dd, NN)))
-            flat = dot(k_blk, ds_half, TN)
-            both = jnp.concatenate([flat[:HEAD_DIM, :BLK], flat[HEAD_DIM:, BLK:]], axis=0)
-            dq_ref[mine, cols] = (jnp.transpose(both) * scale).astype(BF16)
-        for i, (back, mine_ref) in enumerate(((back_k, own_k), (back_v, own_v))):
-            a, b = grads[0][i], grads[1][i]
-            back[p, 0:BLK, :] = a[:BLK].astype(BF16)
-            back[p, BLK:REACH, :] = (a[BLK:REACH] + b[: REACH - BLK]).astype(BF16)
-            mine_ref[p, 0:BLK, :] = a[REACH:] + b[REACH - BLK : REACH]
-            mine_ref[p, BLK:rows, :] = b[REACH:]
-
-        if p < pairs - held:
-            send_back(p)
+            halo_copy(p).wait_recv()
+
+        (s0, k0, v0, q0), (s1, k1, v1, q1) = (
+            tile_grads(
+                p, half, False,
+                grown_ref[p, places[half], :], dprob_ref[p, places[half], :],
+                local_stats, left_stats,
+            )
+            for half in range(2)
+        )
+        square = jnp.concatenate(
+            [
+                square_ref[p, :BLK, :],
+                square_ref[p, BLK:REACH, :] + s1[:BLK],
+                s0 + s1[BLK:],
+            ],
+            axis=0,
+        )
         for lane in range(2):
-            s, t = diagonals(square_ref[:, lane * BLK : (lane + 1) * BLK])
+            s, t = diagonals(square[:, lane * BLK : (lane + 1) * BLK])
             sums.append(s)
             tops.append(t)
+        for out, ref, a, b in ((dk_ref, own_k, k0, k1), (dv_ref, own_v, v0, v1)):
+            out[:BLK, cols] = (ref[p, :BLK, :] + a + b[:BLK]).astype(BF16)
+            out[BLK:, cols] = (ref[p, BLK:, :] + b[BLK:]).astype(BF16)
+        own_q[p, :BLK, :] = q0
+        own_q[p, BLK:, :] = q1
+
+    lag = 1
+    for p in range(pairs + lag):
+        if p < pairs:
+            halo(p)
+        if p >= lag:
+            local(p - lag)
 
     y = jnp.concatenate(sums, axis=0)
     beyond = jnp.sum(
@@ -284,23 +368,23 @@
 
     for k in range(1, sp_size):
         piece_copy(k).start()
-    for p in range(pairs - held, pairs):
-        send_back(p)
+
+    @pl.when(has_right)
+    def _():
+        for p in range(pairs):
+            back_copy(p).start()
 
     def finish(p):
         cols = pl.ds(p * LANES, LANES)
 
-        @pl.when(has_right)
+        @pl.when(has_left)
         def _():
-            for copy in back_copies(p):
-                copy.wait_recv()
-            dk_ref[:, cols] = (own_k[p] + got_k[p].astype(F32)).astype(BF16)
-            dv_ref[:, cols] = (own_v[p] + got_v[p].astype(F32)).astype(BF16)
-
-        @pl.when(jnp.logical_not(has_right))
+            back_copy(p).wait_recv()
+            dq_ref[:, cols] = (own_q[p] + got_q[p].astype(F32)).astype(BF16)
+
+        @pl.when(jnp.logical_not(has_left))
         def _():
-            dk_ref[:, cols] = own_k[p].astype(BF16)
-            dv_ref[:, cols] = own_v[p].astype(BF16)
+            dq_ref[:, cols] = own_q[p].astype(BF16)
 
     total = pieces[me]
     for k in range(1, sp_size):
@@ -321,17 +405,18 @@
     for k in range(1, tp_size):
         share_copy(k).wait_send()
 
+    @pl.when(has_left)
+    def _():
+        local_copy().wait_send()
+        for p in range(pairs):
+            for copy in seq_copies(p):
+                copy.wait_send()
+
     @pl.when(has_right)
     def _():
         for p in range(pairs):
-            for copy in halo_copies(p):
-                copy.wait_send()
-
-    @pl.when(has_left)
-    def _():
-        for p in range(pairs):
-            for copy in back_copies(p):
-                copy.wait_send()
+            halo_copy(p).wait_send()
+            back_copy(p).wait_send()
 
 
 def shards(sp_size, tp_size, query_rows, key_rows, value_rows, out_grad, rel_bias):
@@ -349,18 +434,23 @@
         in_specs=[pl.BlockSpec(memory_space=pltpu.HBM)] * 5,
         out_specs=tuple([pl.BlockSpec(memory_space=pltpu.VMEM)] * 4),
         scratch_shapes=[
+            pltpu.VMEM((2 * rows, width), BF16),
+            pltpu.VMEM((2 * rows, width), BF16),
             pltpu.VMEM((rows, width), BF16),
             pltpu.VMEM((rows, width), BF16),
-            pltpu.VMEM((REACH + rows, width), BF16),
-            pltpu.VMEM((REACH + rows, width), BF16),
-            pltpu.VMEM((pairs, 2, BAND, 2 * BLK), F32),
-            pltpu.VMEM((BAND, 2 * BLK), F32),
+            pltpu.VMEM((pairs, BAND, 2 * BLK), F32),
+            pltpu.VMEM((pairs, REACH, 2 * BLK), F32),
+            pltpu.VMEM((pairs, BAND, 2 * BLK), F32),
+            pltpu.VMEM((pairs, BAND, 2 * BLK), F32),
             pltpu.VMEM((pairs, rows, LANES), F32),
             pltpu.VMEM((pairs, rows, LANES), F32),
-            pltpu.VMEM((pairs, REACH, LANES), BF16),
-            pltpu.VMEM((pairs, REACH, LANES), BF16),
-            pltpu.VMEM((pairs, REACH, LANES), BF16),
-            pltpu.VMEM((pairs, REACH, LANES), BF16),
+            pltpu.VMEM((pairs, rows, LANES), F32),
+            pltpu.VMEM((pairs, rows, LANES), BF16),
+            pltpu.VMEM((pairs, rows, LANES), BF16),
+            pltpu.VMEM((pairs, 8, 2 * BLK), F32),
+            pltpu.VMEM((pairs, 8, 2 * BLK), F32),
+            pltpu.VMEM((pairs, 8, 2 * BLK), F32),
+            pltpu.VMEM((pairs, 8, 2 * BLK), F32),
             pltpu.VMEM(rel_bias.shape[::-1], F32),
             pltpu.VMEM((sp_size, heads, BLK), F32),
             pltpu.VMEM((sp_size - 1, heads, BLK), F32),
@@ -368,8 +458,12 @@
             dma((5,)),
             dma((pairs, 2)),
             dma((pairs, 2)),
-            dma((pairs, 2)),
-            dma((pairs, 2)),
+            dma,
+            dma,
+            dma((pairs,)),
+            dma((pairs,)),
+            dma((pairs,)),
+            dma((pairs,)),
             dma((sp_size - 1,)),
             dma((sp_size - 1,)),
             dma((tp_size - 1,)),

time: 35.3 us -> 34.2 us (0.969)
  Pallas kernels: 34.5 us -> 33.4 us
    pallas_call x1, Pallas kernels: 33.6 us -> 32.5 us  [shards(): pl.pallas_call(partial(kernel, sp_size, tp_size), out_shape=shapes, in_sp...]
where the time goes in v3:
time: 34.2 us; the launch traced here: 34.1 us
  Pallas kernels  33.4 us (98%)
  between operations  0.64 us (2%)
    pallas_call x1, Pallas kernels, shards(): pl.pallas_call(partial(kernel, sp_size, tp_size), out_shape=shapes, in_sp...  32.5 us
    pallas_call x1, Pallas kernels, shards(): pl.pallas_call(write_out, out_shape=shapes, in_specs=[pl.BlockSpec(memory...  0.91 us

profile of v3, /device:TPU:0, one launch (start us, length us, event | category | flops | bytes accessed | tf_op | source)
XLA Modules:
  0.0 34.1 jit_solution(826500275978368189)
XLA Ops:
  0.6 32.5 %shard_map.84 = (bf16[256,512]{1,0:T(8,128)(2,1)S(1)}, bf16[256,512]{1,0:T(8,128)(2,1)S(1)}, bf16[256,512]{1,0:T(8,128)(2,1)S(1)}, f32[32,32]{1,0:T(8,128)S(1)}) custom-call(bf16[256,512]{1,0:T(8,128)(2,1)} %q_hbm.1, bf16[256,512]{1,0:T(8,128)(2,1)} %k_hbm.1, bf16[256,512]{1,0:T(8,128)(2,1)} %v_hbm.1, bf16[256,512]{1,0:T(8,128)(2,1)} %d_hbm.1, f32[32,256]{1,0:T(8,128)} %bitcast.1), custom_call_target="tpu_custom_call" | custom-call | tf_op jit(solution)/shard_map/pallas_call | solution.py:431
  33.1 0.9 %shard_map.85 = (bf16[256,512]{1,0:T(8,128)(2,1)}, bf16[256,512]{1,0:T(8,128)(2,1)}, bf16[256,512]{1,0:T(8,128)(2,1)}, f32[32,32]{1,0:T(8,128)}) custom-call(bf16[256,512]{1,0:T(8,128)(2,1)S(1)} %get-tuple-element.8.refs_0_, bf16[256,512]{1,0:T(8,128)(2,1)S(1)} %get-tuple-element.9.refs_1_, bf16[256,512]{1,0:T(8,128)(2,1)S(1)} %get-tuple-element.10.refs_2_, ...), custom_call_target="tpu_custom_call" | custom-call | tf_op jit(solution)/shard_map/pallas_call | solution.py:476

commit v4 on v3

--- a/solution.py
+++ b/solution.py
@@ -316,7 +316,7 @@
         own_q[p, :BLK, :] = q0
         own_q[p, BLK:, :] = q1
 
-    lag = 1
+    lag = pairs
     for p in range(pairs + lag):
         if p < pairs:
             halo(p)

time: 34.2 us -> 32.1 us (0.939)
  Pallas kernels: 33.4 us -> 31.3 us
    pallas_call x1, Pallas kernels: 32.5 us -> 30.3 us  [shards(): pl.pallas_call(partial(kernel, sp_size, tp_size), out_shape=shapes, in_sp...]
where the time goes in v4:
time: 32.1 us; the launch traced here: 31.9 us
  Pallas kernels  31.3 us (98%)
  between operations  0.64 us (2%)
    pallas_call x1, Pallas kernels, shards(): pl.pallas_call(partial(kernel, sp_size, tp_size), out_shape=shapes, in_sp...  30.3 us
    pallas_call x1, Pallas kernels, shards(): pl.pallas_call(write_out, out_shape=shapes, in_specs=[pl.BlockSpec(memory...  0.91 us

profile of v4, /device:TPU:0, one launch (start us, length us, event | category | flops | bytes accessed | tf_op | source)
XLA Modules:
  0.0 31.9 jit_solution(12682780616451893309)
XLA Ops:
  0.6 30.3 %shard_map.84 = (bf16[256,512]{1,0:T(8,128)(2,1)S(1)}, bf16[256,512]{1,0:T(8,128)(2,1)S(1)}, bf16[256,512]{1,0:T(8,128)(2,1)S(1)}, f32[32,32]{1,0:T(8,128)S(1)}) custom-call(bf16[256,512]{1,0:T(8,128)(2,1)} %q_hbm.1, bf16[256,512]{1,0:T(8,128)(2,1)} %k_hbm.1, bf16[256,512]{1,0:T(8,128)(2,1)} %v_hbm.1, bf16[256,512]{1,0:T(8,128)(2,1)} %d_hbm.1, f32[32,256]{1,0:T(8,128)} %bitcast.1), custom_call_target="tpu_custom_call" | custom-call | tf_op jit(solution)/shard_map/pallas_call | solution.py:431
  31.0 0.9 %shard_map.85 = (bf16[256,512]{1,0:T(8,128)(2,1)}, bf16[256,512]{1,0:T(8,128)(2,1)}, bf16[256,512]{1,0:T(8,128)(2,1)}, f32[32,32]{1,0:T(8,128)}) custom-call(bf16[256,512]{1,0:T(8,128)(2,1)S(1)} %get-tuple-element.8.refs_0_, bf16[256,512]{1,0:T(8,128)(2,1)S(1)} %get-tuple-element.9.refs_1_, bf16[256,512]{1,0:T(8,128)(2,1)S(1)} %get-tuple-element.10.refs_2_, ...), custom_call_target="tpu_custom_call" | custom-call | tf_op jit(solution)/shard_map/pallas_call | solution.py:476
